TPU v7x, 32 devices: a whole 2x2x4 slice. The times are simulated.
32 devices in a mesh: sp: 4 (over z), dp: 8 (over y, x, core).
Axes of the slice: x: 2, y: 2, z: 4, core: 2. Of those that a mesh axis runs over, the one named last changes fastest.
Arguments:
- tokens: bfloat16 [16, 256, 1024], P('dp', 'sp'), may hold values from -6 to 6
- norm_gain: float32 [1024], replicated, may hold values from 0.1 to 1.9
- w_query: bfloat16 [1024, 128], P('dp'), may hold values from -0.1875 to 0.1875
- w_key: bfloat16 [1024, 128], P('dp'), may hold values from -0.1875 to 0.1875
- w_value: bfloat16 [1024, 128], P('dp'), may hold values from -0.1875 to 0.1875
- w_rank_forward: bfloat16 [1024, 16], P('dp'), may hold values from -0.1875 to 0.1875
- w_rank_backward: bfloat16 [1024, 16], P('dp'), may hold values from -0.1875 to 0.1875
- up_forward: bfloat16 [16, 128], replicated, may hold values from -1.5 to 1.5
- up_backward: bfloat16 [16, 128], replicated, may hold values from -1.5 to 1.5
- bias_forward: float32 [128], replicated, may hold values from -1.5 to 3
- bias_backward: float32 [128], replicated, may hold values from -1.5 to 3
- out_gain: float32 [32], replicated, may hold values from 0.1 to 1.9
- w_out: bfloat16 [128, 1024], P('dp'), may hold values from -0.5 to 0.5
Outputs:
- mixed_out: bfloat16 [16, 256, 1024], P('dp', 'sp')
All inputs are finite; a program needn't handle non-finite values.
Results may differ from a plain program's by a relative error of at most 0.005.
Values may be sent and summed in bfloat16 or wider, within the bound.
A program may use at most 64 MiB of HBM per device.

v0:
```python
import jax
import jax.numpy as jnp
from jax import lax
from jax.sharding import PartitionSpec as P

HK = 32
HV = 32
BLOCK = 64
eps = 1e-06
precise = lax.Precision.HIGHEST


def over_all(x, axis, dim, take_in, carry):
    whole = jax.tree.map(lambda part: lax.all_gather(part, axis, axis=dim, tiled=True), x)
    return take_in(carry, whole, jnp.int32(0))


def for_sending(x):
    return jax.tree.map(lambda a: a.astype(jnp.bfloat16) if a.dtype == jnp.float32 else a, x)


def rms_norm(values, norm_scale):
    return values * lax.rsqrt(jnp.mean(values * values, axis=-1, keepdims=True) + eps) * norm_scale


def one_way(queries, key_rows, value_rows, decay_rates):
    head_count, length, key_width = queries.shape
    value_width = value_rows.shape[-1]
    blocks = length // BLOCK

    def in_blocks(tensor):
        return tensor.reshape(head_count, blocks, BLOCK, tensor.shape[-1])

    query_blocks = in_blocks(queries)
    key_blocks = in_blocks(key_rows)
    value_blocks = in_blocks(value_rows)
    running = jnp.cumsum(in_blocks(decay_rates), axis=2)
    closing = running[:, :, -1:, :]
    query_decayed = query_blocks * jnp.exp(running)
    key_inverse = key_blocks * jnp.exp(-running)
    key_remain = key_blocks * jnp.exp(closing - running)
    triangle = jnp.tril(jnp.ones((BLOCK, BLOCK), jnp.float32))
    scores = jnp.einsum("hnid,hnjd->hnij", query_decayed, key_inverse, precision=precise) * triangle
    within = jnp.einsum("hnij,hnjv->hniv", scores, value_blocks, precision=precise)
    block_decay = jnp.exp(closing[:, :, 0, :])

    def advance(carried, inputs):
        query_now, key_now, value_now, decay_now = inputs
        emitted = jnp.einsum("hid,hdv->hiv", query_now, carried, precision=precise)
        carried = decay_now[..., None] * carried + jnp.einsum(
            "hid,hiv->hdv", key_now, value_now, precision=precise
        )
        return (carried, emitted)

    initial = jnp.zeros((head_count, key_width, value_width), jnp.float32)
    stacked = tuple(
        (
            jnp.moveaxis(tensor, 1, 0)
            for tensor in (query_decayed, key_remain, value_blocks, block_decay)
        )
    )
    final_state, across = lax.scan(advance, initial, stacked)
    return (within + jnp.moveaxis(across, 0, 1)).reshape(head_count, length, value_width)


def both_ways(queries, key_rows, value_rows, rates_forward, rates_backward):
    forward = one_way(queries, key_rows, value_rows, rates_forward)
    backward = one_way(
        jnp.flip(queries, 1),
        jnp.flip(key_rows, 1),
        jnp.flip(value_rows, 1),
        jnp.flip(rates_backward, 1),
    )
    return forward + jnp.flip(backward, 1)


def by_head(tensor, head_width):
    length = tensor.shape[0]
    return tensor.reshape(length, -1, head_width).transpose(1, 0, 2).astype(jnp.float32)


def attend(queries, key_rows, value_rows, rates_forward, rates_backward, out_gain):
    combined = both_ways(
        by_head(queries, HK) * HK ** (-0.5),
        by_head(key_rows, HK),
        by_head(value_rows, HV),
        by_head(rates_forward, HK),
        by_head(rates_backward, HK),
    )
    normed = rms_norm(combined, out_gain).astype(jnp.bfloat16)
    return normed.transpose(1, 0, 2).reshape(normed.shape[1], -1)


def per_device(
    tokens,
    norm_gain,
    w_query,
    w_key,
    w_value,
    w_rank_forward,
    w_rank_backward,
    up_forward,
    up_backward,
    bias_forward,
    bias_backward,
    out_gain,
    w_out,
):
    seq_local, tok_local, model_width = tokens.shape
    sp_count = lax.axis_size("sp")
    length = tok_local * sp_count
    rate_scale = 2.0 / length
    row_count = seq_local * tok_local
    normed = rms_norm(tokens.reshape(row_count, model_width).astype(jnp.float32), norm_gain).astype(
        jnp.bfloat16
    )

    def add_rows(totals, pieces, offset):
        span_rows = pieces[0].shape[0]
        left_part = lax.dynamic_slice_in_dim(normed, offset, span_rows, 1)
        return tuple(
            (
                running_sum + jnp.dot(left_part, shard_piece, preferred_element_type=jnp.float32)
                for running_sum, shard_piece in zip(totals, pieces)
            )
        )

    starting = tuple(
        (
            jnp.zeros((row_count, weight.shape[1]), jnp.float32)
            for weight in (w_query, w_key, w_value, w_rank_forward, w_rank_backward)
        )
    )
    projected = over_all(
        (w_query, w_key, w_value, w_rank_forward, w_rank_backward), "dp", 0, add_rows, starting
    )
    queries = projected[0].astype(jnp.bfloat16).reshape(seq_local, tok_local, -1)
    key_rows = projected[1].astype(jnp.bfloat16).reshape(seq_local, tok_local, -1)
    value_rows = projected[2].astype(jnp.bfloat16).reshape(seq_local, tok_local, -1)
    rank_forward = projected[3].astype(jnp.bfloat16)
    rank_backward = projected[4].astype(jnp.bfloat16)
    head_queries, head_keys, head_values = (
        lax.all_to_all(queries, "sp", split_axis=2, concat_axis=1, tiled=True),
        lax.all_to_all(key_rows, "sp", split_axis=2, concat_axis=1, tiled=True),
        lax.all_to_all(value_rows, "sp", split_axis=2, concat_axis=1, tiled=True),
    )
    own_forward = (
        jax.nn.log_sigmoid(
            jnp.dot(rank_forward, up_forward, preferred_element_type=jnp.float32) + bias_forward
        )
        * rate_scale
    )
    own_backward = (
        jax.nn.log_sigmoid(
            jnp.dot(rank_backward, up_backward, preferred_element_type=jnp.float32) + bias_backward
        )
        * rate_scale
    )
    rates_forward, rates_backward = (
        lax.all_to_all(
            for_sending(own_forward.reshape(seq_local, tok_local, -1)),
            "sp",
            split_axis=2,
            concat_axis=1,
            tiled=True,
        ),
        lax.all_to_all(
            for_sending(own_backward.reshape(seq_local, tok_local, -1)),
            "sp",
            split_axis=2,
            concat_axis=1,
            tiled=True,
        ),
    )
    attended = jax.vmap(attend, in_axes=(0, 0, 0, 0, 0, None))(
        head_queries, head_keys, head_values, rates_forward, rates_backward, out_gain
    )
    gathered_heads = jax.tree.map(
        lambda part, own: part.astype(own.dtype),
        lax.all_to_all(for_sending(attended), "sp", split_axis=1, concat_axis=2, tiled=True),
        attended,
    ).reshape(row_count, -1)

    def add_out(running_sum, shard_piece, offset):
        left_part = lax.dynamic_slice_in_dim(gathered_heads, offset, shard_piece.shape[0], 1)
        return running_sum + jnp.dot(left_part, shard_piece, preferred_element_type=jnp.float32)

    mixed_out = over_all(
        w_out, "dp", 0, add_out, jnp.zeros((row_count, w_out.shape[1]), jnp.float32)
    )
    return mixed_out.astype(jnp.bfloat16).reshape(seq_local, tok_local, -1)


def solution(mesh):
    return jax.shard_map(
        per_device,
        mesh=mesh,
        in_specs=(
            P("dp", "sp", None),
            P(),
            P("dp", None),
            P("dp", None),
            P("dp", None),
            P("dp", None),
            P("dp", None),
            P(),
            P(),
            P(),
            P(),
            P(),
            P("dp", None),
        ),
        out_specs=P("dp", "sp", None),
        check_vma=False,
    )
```

profile of v0, /device:TPU:0, one launch (start us, length us, event | category | flops | bytes accessed | tf_op | source)
XLA Modules:
  0.0 118.0 jit_solution(11206527147901036018)
XLA Ops:
  0.0 1.2 multiply_reduce_fusion
  1.3 11.1 %all_gather.18 = bf16[1024,128]{1,0:T(8,128)(2,1)S(1)} all-gather(bf16[128,128]{1,0:T(8,128)(2,1)} %param.19), channel_id=1, replica_groups=mesh['sp'=4,'dp'=8] {'dp'}, dimensions={0}, use_global_device_ids=true | all-gather | bytes 294912 | tf_op jit(solution)/shard_map/all_gather | solution.py:14
  12.9 0.7 reshape.393
  13.6 5.0 %all-to-all-start = ((bf16[4,2,2048]{2,1,0:T(2,128)(2,1)}), bf16[4,2,2048]{2,1,0:T(2,128)(2,1)S(1)}, u32[]{:S(2)}, u32[]{:S(2)}) async-start(bf16[4,2,2048]{2,1,0:T(2,128)(2,1)} %reshape.393), calls=%async_computation | async-start | bytes 65536 | tf_op jit(solution)/shard_map/all_to_all | solution.py:143
  18.6 9.0 %all_gather.20 = bf16[1024,128]{1,0:T(8,128)(2,1)S(1)} all-gather(bf16[128,128]{1,0:T(8,128)(2,1)S(1)} %copy-done.2), channel_id=1, replica_groups=mesh['sp'=4,'dp'=8] {'dp'}, dimensions={0}, use_global_device_ids=true | all-gather | bytes 294912 | tf_op jit(solution)/shard_map/all_gather | solution.py:14
  27.9 0.5 copy-done.6
  28.3 8.2 %all_gather.19 = bf16[1024,16]{0,1:T(8,128)(2,1)S(1)} all-gather(bf16[128,16]{0,1:T(8,128)(2,1)S(1)} %copy-done.6), channel_id=1, replica_groups=mesh['sp'=4,'dp'=8] {'dp'}, dimensions={0}, use_global_device_ids=true | all-gather | bytes 36864 | tf_op jit(solution)/shard_map/all_gather | solution.py:14
  36.6 9.0 %all_gather.21 = bf16[1024,128]{1,0:T(8,128)(2,1)S(1)} all-gather(bf16[128,128]{1,0:T(8,128)(2,1)S(1)} %copy-done.3), channel_id=1, replica_groups=mesh['sp'=4,'dp'=8] {'dp'}, dimensions={0}, use_global_device_ids=true | all-gather | bytes 294912 | tf_op jit(solution)/shard_map/all_gather | solution.py:14
  45.9 0.5 copy-done.7
  46.3 8.2 %all_gather.22 = bf16[1024,16]{0,1:T(8,128)(2,1)S(1)} all-gather(bf16[128,16]{0,1:T(8,128)(2,1)S(1)} %copy-done.7), channel_id=1, replica_groups=mesh['sp'=4,'dp'=8] {'dp'}, dimensions={0}, use_global_device_ids=true | all-gather | bytes 36864 | tf_op jit(solution)/shard_map/all_gather | solution.py:14
  55.8 0.7 reshape.389
  56.7 0.7 reshape.391
  57.5 0.7 reshape.387
  58.4 0.7 reshape.395
  59.1 5.1 %all-to-all-start.1 = ((bf16[4,2,2048]{2,1,0:T(2,128)(2,1)}), bf16[4,2,2048]{2,1,0:T(2,128)(2,1)S(1)}, u32[]{:S(2)}, u32[]{:S(2)}) async-start(bf16[4,2,2048]{2,1,0:T(2,128)(2,1)} %reshape.391), calls=%async_computation.1 | async-start | bytes 65536 | tf_op jit(solution)/shard_map/all_to_all | solution.py:160
  64.3 5.5 %all-to-all-done.1 = bf16[4,2,2048]{2,1,0:T(2,128)(2,1)S(1)} async-done(((bf16[4,2,2048]{2,1,0:T(2,128)(2,1)}), bf16[4,2,2048]{2,1,0:T(2,128)(2,1)S(1)}, u32[]{:S(2)}, u32[]{:S(2)}) %all-to-all-start.1) | async-done | bytes 32800 | tf_op jit(solution)/shard_map/all_to_all | solution.py:160
  69.9 3.3 %all-to-all-start.2 = ((bf16[4,2,2048]{2,1,0:T(2,128)(2,1)}), bf16[4,2,2048]{2,1,0:T(2,128)(2,1)S(1)}, u32[]{:S(2)}, u32[]{:S(2)}) async-start(bf16[4,2,2048]{2,1,0:T(2,128)(2,1)} %reshape.389), calls=%async_computation.2 | async-start | bytes 65536 | tf_op jit(solution)/shard_map/all_to_all | solution.py:144
  73.3 5.5 %all-to-all-done.2 = bf16[4,2,2048]{2,1,0:T(2,128)(2,1)S(1)} async-done(((bf16[4,2,2048]{2,1,0:T(2,128)(2,1)}), bf16[4,2,2048]{2,1,0:T(2,128)(2,1)S(1)}, u32[]{:S(2)}, u32[]{:S(2)}) %all-to-all-start.2) | async-done | bytes 32800 | tf_op jit(solution)/shard_map/all_to_all | solution.py:144
  78.8 3.3 %all-to-all-start.3 = ((bf16[4,2,2048]{2,1,0:T(2,128)(2,1)}), bf16[4,2,2048]{2,1,0:T(2,128)(2,1)S(1)}, u32[]{:S(2)}, u32[]{:S(2)}) async-start(bf16[4,2,2048]{2,1,0:T(2,128)(2,1)} %reshape.387), calls=%async_computation.3 | async-start | bytes 65536 | tf_op jit(solution)/shard_map/all_to_all | solution.py:145
  82.6 5.1 %all-to-all-done.3 = bf16[4,2,2048]{2,1,0:T(2,128)(2,1)S(1)} async-done(((bf16[4,2,2048]{2,1,0:T(2,128)(2,1)}), bf16[4,2,2048]{2,1,0:T(2,128)(2,1)S(1)}, u32[]{:S(2)}, u32[]{:S(2)}) %all-to-all-start.3) | async-done | bytes 32800 | tf_op jit(solution)/shard_map/all_to_all | solution.py:145
  87.7 3.3 %all-to-all-start.4 = ((bf16[4,2,2048]{2,1,0:T(2,128)(2,1)}), bf16[4,2,2048]{2,1,0:T(2,128)(2,1)S(1)}, u32[]{:S(2)}, u32[]{:S(2)}) async-start(bf16[4,2,2048]{2,1,0:T(2,128)(2,1)} %reshape.395), calls=%async_computation.4 | async-start | bytes 65536 | tf_op jit(solution)/shard_map/all_to_all | solution.py:167
  91.3 0.6 convolution_multiply_fusion.1
  92.3 1.8 %while.26 = (s32[]{:T(128)}, f32[2,1,32,32]{3,2,0,1:T(8,128)S(1)}, f32[4,2,1,64,32]{3,4,0,1,2:T(8,128)S(1)}, f32[4,2,1,32]{3,0,1,2:T(4,128)S(1)}, f32[4,2,1,64,3...) while((s32[]{:T(128)}, f32[2,1,32,32]{3,2,0,1:T(8,128)S(1)}, ...), condition=%wide.region_3.4_spmd.clone, body=%wide.region_2.3_spmd.clone.sunk | while | flops 3153923 | bytes 209522 | solution.py:62
  95.9 0.6 all-to-all-done.4
  97.9 2.0 %while.27 = (s32[]{:T(128)}, f32[2,1,32,32]{3,2,0,1:T(8,128)S(1)}, f32[4,2,1,64,32]{3,4,0,1,2:T(8,128)S(1)}, f32[4,2,1,32]{3,0,1,2:T(4,128)S(1)}, f32[4,2,1,64,3...) while((s32[]{:T(128)}, f32[2,1,32,32]{3,2,0,1:T(8,128)S(1)}, ...), condition=%wide.region_6.7_spmd.clone, body=%wide.region_5.6_spmd.clone.sunk | while | flops 3153923 | bytes 240763 | solution.py:62
  99.8 0.6 convolution_multiply_fusion
  100.4 0.5 fusion.29
  101.4 0.6 copy-done.8
  102.3 0.8 reshape.397
  103.1 4.6 %all-to-all-start.5 = ((bf16[4,2,2048]{2,1,0:T(2,128)(2,1)}), bf16[4,2,2048]{2,1,0:T(2,128)(2,1)S(1)}, u32[]{:S(2)}, u32[]{:S(2)}) async-start(bf16[4,2,2048]{2,1,0:T(2,128)(2,1)} %reshape.397), calls=%async_computation.5 | async-start | bytes 65536 | tf_op jit(solution)/shard_map/all_to_all | solution.py:180
  107.7 9.0 %all_gather.23 = bf16[128,1024]{1,0:T(8,128)(2,1)S(1)} all-gather(bf16[16,1024]{1,0:T(8,128)(2,1)S(1)} %copy-done.4), channel_id=1, replica_groups=mesh['sp'=4,'dp'=8] {'dp'}, dimensions={0}, use_global_device_ids=true | all-gather | bytes 294912 | tf_op jit(solution)/shard_map/all_gather | solution.py:14
  117.1 1.0 convolution_convert_fusion
  (124 shorter events, 11.5 us)
Async XLA Ops:
  0.0 54.5 %copy-start = (bf16[16,128]{1,0:T(8,128)(2,1)S(1)}, bf16[16,128]{1,0:T(8,128)(2,1)}, u32[]{:S(2)}) copy-start(bf16[16,128]{1,0:T(8,128)(2,1)} %param.24) | copy-start | bytes 12292
  0.0 12.4 %copy-start.1 = (bf16[2,64,1024]{2,1,0:T(8,128)(2,1)S(1)}, bf16[2,64,1024]{2,1,0:T(8,128)(2,1)}, u32[]{:S(2)}) copy-start(bf16[2,64,1024]{2,1,0:T(8,128)(2,1)} %param.17) | copy-start | bytes 786436
  1.3 11.1 %copy-start.5 = (f32[1024]{0:T(1024)S(1)}, f32[1024]{0:T(1024)}, u32[]{:S(2)}) copy-start(f32[1024]{0:T(1024)} %param.18) | copy-start | bytes 12292
  13.6 5.0 %copy-start.2 = (bf16[128,128]{1,0:T(8,128)(2,1)S(1)}, bf16[128,128]{1,0:T(8,128)(2,1)}, u32[]{:S(2)}) copy-start(bf16[128,128]{1,0:T(8,128)(2,1)} %param.20) | copy-start | bytes 98308
  13.6 45.5 %all-to-all-start = ((bf16[4,2,2048]{2,1,0:T(2,128)(2,1)}), bf16[4,2,2048]{2,1,0:T(2,128)(2,1)S(1)}, u32[]{:S(2)}, u32[]{:S(2)}) async-start(bf16[4,2,2048]{2,1,0:T(2,128)(2,1)} %reshape.393), calls=%async_computation | async-start | bytes 65536 | tf_op jit(solution)/shard_map/all_to_all | solution.py:143
  27.7 0.7 copy-start.6
  28.3 8.2 %copy-start.3 = (bf16[128,128]{1,0:T(8,128)(2,1)S(1)}, bf16[128,128]{1,0:T(8,128)(2,1)}, u32[]{:S(2)}) copy-start(bf16[128,128]{1,0:T(8,128)(2,1)} %param.21) | copy-start | bytes 98308
  45.6 0.7 copy-start.7
  46.3 8.2 %copy-start.10 = (f32[128]{0:T(128)S(1)}, f32[128]{0:T(128)}, u32[]{:S(2)}) copy-start(f32[128]{0:T(128)} %param.26) | copy-start | bytes 1540
  54.6 0.7 copy-start.9
  54.6 0.7 copy-start.11
  59.1 10.7 %all-to-all-start.1 = ((bf16[4,2,2048]{2,1,0:T(2,128)(2,1)}), bf16[4,2,2048]{2,1,0:T(2,128)(2,1)S(1)}, u32[]{:S(2)}, u32[]{:S(2)}) async-start(bf16[4,2,2048]{2,1,0:T(2,128)(2,1)} %reshape.391), calls=%async_computation.1 | async-start | bytes 65536 | tf_op jit(solution)/shard_map/all_to_all | solution.py:160
  69.9 8.9 %all-to-all-start.2 = ((bf16[4,2,2048]{2,1,0:T(2,128)(2,1)}), bf16[4,2,2048]{2,1,0:T(2,128)(2,1)S(1)}, u32[]{:S(2)}, u32[]{:S(2)}) async-start(bf16[4,2,2048]{2,1,0:T(2,128)(2,1)} %reshape.389), calls=%async_computation.2 | async-start | bytes 65536 | tf_op jit(solution)/shard_map/all_to_all | solution.py:144
  78.8 8.9 %all-to-all-start.3 = ((bf16[4,2,2048]{2,1,0:T(2,128)(2,1)}), bf16[4,2,2048]{2,1,0:T(2,128)(2,1)S(1)}, u32[]{:S(2)}, u32[]{:S(2)}) async-start(bf16[4,2,2048]{2,1,0:T(2,128)(2,1)} %reshape.387), calls=%async_computation.3 | async-start | bytes 65536 | tf_op jit(solution)/shard_map/all_to_all | solution.py:145
  87.7 8.9 %all-to-all-start.4 = ((bf16[4,2,2048]{2,1,0:T(2,128)(2,1)}), bf16[4,2,2048]{2,1,0:T(2,128)(2,1)S(1)}, u32[]{:S(2)}, u32[]{:S(2)}) async-start(bf16[4,2,2048]{2,1,0:T(2,128)(2,1)} %reshape.395), calls=%async_computation.4 | async-start | bytes 65536 | tf_op jit(solution)/shard_map/all_to_all | solution.py:167
  101.4 0.7 copy-start.8
  103.1 4.6 %copy-start.4 = (bf16[16,1024]{1,0:T(8,128)(2,1)S(1)}, bf16[16,1024]{1,0:T(8,128)(2,1)}, u32[]{:S(2)}) copy-start(bf16[16,1024]{1,0:T(8,128)(2,1)} %param.29) | copy-start | bytes 98308
  103.1 13.7 %all-to-all-start.5 = ((bf16[4,2,2048]{2,1,0:T(2,128)(2,1)}), bf16[4,2,2048]{2,1,0:T(2,128)(2,1)S(1)}, u32[]{:S(2)}, u32[]{:S(2)}) async-start(bf16[4,2,2048]{2,1,0:T(2,128)(2,1)} %reshape.397), calls=%async_computation.5 | async-start | bytes 65536 | tf_op jit(solution)/shard_map/all_to_all | solution.py:180
where the time goes:
time: 119 us; the launch traced here: 118 us
  blocking collectives  54.7 us (46%)
  starting transfers between devices  24.5 us (21%)
  waiting for transfers between devices  16.7 us (14%)
  local copies, waits for them, and re-layouts  11.5 us (10%)
  matrix products  7.71 us (6%)
  other arithmetic  2.15 us (2%)
    all_gather x6, blocking collectives, over_all(): lax.all_gather(part, axis, axis=dim, tiled=True)  54.7 us
    unnamed x40, local copies, waits for them, and re-layouts  7.46 us
    all_to_all x1, waiting for transfers between devices, per_device(): lax.all_to_all(for_sending(own_forward.reshape(seq_local, tok_local, -1))...  5.52 us
    all_to_all x1, waiting for transfers between devices, per_device(): lax.all_to_all(key_rows, 'sp', split_axis=2, concat_axis=1, tiled=True)  5.47 us
    all_to_all x1, starting transfers between devices, per_device(): lax.all_to_all(for_sending(own_forward.reshape(seq_local, tok_local, -1))...  5.09 us
    all_to_all x1, waiting for transfers between devices, per_device(): lax.all_to_all(value_rows, 'sp', split_axis=2, concat_axis=1, tiled=True)  5.08 us
    all_to_all x1, starting transfers between devices, per_device(): lax.all_to_all(queries, 'sp', split_axis=2, concat_axis=1, tiled=True)  5 us
    all_to_all x1, starting transfers between devices, per_device(): lax.all_to_all(for_sending(attended), 'sp', split_axis=1, concat_axis=2,...  4.59 us
  transfers between devices with their start and end apart: 6, of which 4 were waited for; matrix products, arithmetic and copies ran while one was open for 9% of the time, Pallas kernels for 0%

commit v1 on v0

--- a/solution.py
+++ b/solution.py
@@ -141,7 +141,10 @@
     rank_backward = projected[4].astype(jnp.bfloat16)
     head_queries, head_keys, head_values = (
         lax.all_to_all(queries, "sp", split_axis=2, concat_axis=1, tiled=True),
-        lax.all_to_all(key_rows, "sp", split_axis=2, concat_axis=1, tiled=True),
+        jnp.concatenate(
+            lax.all_to_all(jnp.stack(jnp.split(key_rows, lax.axis_size("sp"), axis=2)), "sp", 0, 0),
+            axis=1,
+        ),
         lax.all_to_all(value_rows, "sp", split_axis=2, concat_axis=1, tiled=True),
     )
     own_forward = (

time: 119 us -> 120 us (level)
    unnamed x40 -> x42, local copies, waits for them, and re-layouts: 7.46 us -> 7.82 us
where the time goes in v1:
time: 120 us; the launch traced here: 119 us
  blocking collectives  54.7 us (46%)
  starting transfers between devices  24.4 us (20%)
  waiting for transfers between devices  16.6 us (14%)
  local copies, waits for them, and re-layouts  12.1 us (10%)
  matrix products  7.73 us (6%)
  other arithmetic  2.21 us (2%)
    all_gather x6, blocking collectives, over_all(): lax.all_gather(part, axis, axis=dim, tiled=True)  54.7 us
    unnamed x42, local copies, waits for them, and re-layouts  7.82 us
    all_to_all x1, waiting for transfers between devices, per_device(): lax.all_to_all(for_sending(own_forward.reshape(seq_local, tok_local, -1))...  5.5 us
    all_to_all x1, waiting for transfers between devices, per_device(): lax.all_to_all(value_rows, 'sp', split_axis=2, concat_axis=1, tiled=True)  5.33 us
    all_to_all x1, starting transfers between devices, per_device(): lax.all_to_all(for_sending(own_forward.reshape(seq_local, tok_local, -1))...  5.09 us
    all_to_all x1, waiting for transfers between devices, per_device(): lax.all_to_all(jnp.stack(jnp.split(key_rows, lax.axis_size('sp'), axis=2)...  5.07 us
    all_to_all x1, starting transfers between devices, per_device(): lax.all_to_all(queries, 'sp', split_axis=2, concat_axis=1, tiled=True)  5 us
    all_to_all x1, starting transfers between devices, per_device(): lax.all_to_all(for_sending(attended), 'sp', split_axis=1, concat_axis=2,...  4.51 us
  transfers between devices with their start and end apart: 6, of which 4 were waited for; matrix products, arithmetic and copies ran while one was open for 9% of the time, Pallas kernels for 0%

profile of v1, /device:TPU:0, one launch (start us, length us, event | category | flops | bytes accessed | tf_op | source)
XLA Modules:
  0.0 118.5 jit_solution(7105921021685367705)
XLA Ops:
  0.0 1.2 multiply_reduce_fusion
  1.3 11.1 %all_gather.18 = bf16[1024,128]{1,0:T(8,128)(2,1)S(1)} all-gather(bf16[128,128]{1,0:T(8,128)(2,1)} %param.19), channel_id=1, replica_groups=mesh['sp'=4,'dp'=8] {'dp'}, dimensions={0}, use_global_device_ids=true | all-gather | bytes 294912 | tf_op jit(solution)/shard_map/all_gather | solution.py:14
  12.9 0.7 reshape.386
  13.6 5.0 %all-to-all-start = ((bf16[4,2,2048]{2,1,0:T(2,128)(2,1)}), bf16[4,2,2048]{2,1,0:T(2,128)(2,1)S(1)}, u32[]{:S(2)}, u32[]{:S(2)}) async-start(bf16[4,2,2048]{2,1,0:T(2,128)(2,1)} %reshape.386), calls=%async_computation | async-start | bytes 65536 | tf_op jit(solution)/shard_map/all_to_all | solution.py:143
  18.6 8.8 %all_gather.19 = bf16[1024,16]{0,1:T(8,128)(2,1)S(1)} all-gather(bf16[128,16]{0,1:T(8,128)(2,1)S(1)} %copy-done.6), channel_id=1, replica_groups=mesh['sp'=4,'dp'=8] {'dp'}, dimensions={0}, use_global_device_ids=true | all-gather | bytes 36864 | tf_op jit(solution)/shard_map/all_gather | solution.py:14
  27.4 8.5 %all_gather.20 = bf16[1024,128]{1,0:T(8,128)(2,1)S(1)} all-gather(bf16[128,128]{1,0:T(8,128)(2,1)S(1)} %copy-done.2), channel_id=1, replica_groups=mesh['sp'=4,'dp'=8] {'dp'}, dimensions={0}, use_global_device_ids=true | all-gather | bytes 294912 | tf_op jit(solution)/shard_map/all_gather | solution.py:14
  36.6 0.7 copy-done.3
  37.3 9.1 %all_gather.21 = bf16[1024,128]{1,0:T(8,128)(2,1)S(1)} all-gather(bf16[128,128]{1,0:T(8,128)(2,1)S(1)} %copy-done.3), channel_id=1, replica_groups=mesh['sp'=4,'dp'=8] {'dp'}, dimensions={0}, use_global_device_ids=true | all-gather | bytes 294912 | tf_op jit(solution)/shard_map/all_gather | solution.py:14
  46.5 0.5 copy-done.7
  47.0 8.2 %all_gather.22 = bf16[1024,16]{0,1:T(8,128)(2,1)S(1)} all-gather(bf16[128,16]{0,1:T(8,128)(2,1)S(1)} %copy-done.7), channel_id=1, replica_groups=mesh['sp'=4,'dp'=8] {'dp'}, dimensions={0}, use_global_device_ids=true | all-gather | bytes 36864 | tf_op jit(solution)/shard_map/all_gather | solution.py:14
  56.5 0.7 reshape.382
  57.3 0.7 reshape.384
  58.1 0.7 reshape.380
  59.0 0.7 reshape.388
  59.7 5.1 %all-to-all-start.1 = ((bf16[4,2,2048]{2,1,0:T(2,128)(2,1)}), bf16[4,2,2048]{2,1,0:T(2,128)(2,1)S(1)}, u32[]{:S(2)}, u32[]{:S(2)}) async-start(bf16[4,2,2048]{2,1,0:T(2,128)(2,1)} %reshape.382), calls=%async_computation.1 | async-start | bytes 65536 | tf_op jit(solution)/shard_map/all_to_all | solution.py:163
  65.0 5.5 %all-to-all-done.1 = bf16[4,2,2048]{2,1,0:T(2,128)(2,1)S(1)} async-done(((bf16[4,2,2048]{2,1,0:T(2,128)(2,1)}), bf16[4,2,2048]{2,1,0:T(2,128)(2,1)S(1)}, u32[]{:S(2)}, u32[]{:S(2)}) %all-to-all-start.1) | async-done | bytes 32800 | tf_op jit(solution)/shard_map/all_to_all | solution.py:163
  70.5 3.3 %all-to-all-start.3 = ((bf16[4,2,2048]{2,1,0:T(2,128)(2,1)}), bf16[4,2,2048]{2,1,0:T(2,128)(2,1)S(1)}, u32[]{:S(2)}, u32[]{:S(2)}) async-start(bf16[4,2,2048]{2,1,0:T(2,128)(2,1)} %reshape.380), calls=%async_computation.3 | async-start | bytes 65536 | tf_op jit(solution)/shard_map/all_to_all | solution.py:148
  74.0 5.3 %all-to-all-done.3 = bf16[4,2,2048]{2,1,0:T(2,128)(2,1)S(1)} async-done(((bf16[4,2,2048]{2,1,0:T(2,128)(2,1)}), bf16[4,2,2048]{2,1,0:T(2,128)(2,1)S(1)}, u32[]{:S(2)}, u32[]{:S(2)}) %all-to-all-start.3) | async-done | bytes 32800 | tf_op jit(solution)/shard_map/all_to_all | solution.py:148
  79.4 3.3 %all-to-all-start.2 = ((bf16[4,2,2048]{2,1,0:T(2,128)(2,1)}), bf16[4,2,2048]{2,1,0:T(2,128)(2,1)S(1)}, u32[]{:S(2)}, u32[]{:S(2)}) async-start(bf16[4,2,2048]{2,1,0:T(2,128)(2,1)} %reshape.384), calls=%async_computation.2 | async-start | bytes 65536 | tf_op jit(solution)/shard_map/all_to_all | solution.py:145
  83.2 5.1 %all-to-all-done.2 = bf16[4,2,2048]{2,1,0:T(2,128)(2,1)S(1)} async-done(((bf16[4,2,2048]{2,1,0:T(2,128)(2,1)}), bf16[4,2,2048]{2,1,0:T(2,128)(2,1)S(1)}, u32[]{:S(2)}, u32[]{:S(2)}) %all-to-all-start.2) | async-done | bytes 32800 | tf_op jit(solution)/shard_map/all_to_all | solution.py:145
  88.3 3.3 %all-to-all-start.4 = ((bf16[4,2,2048]{2,1,0:T(2,128)(2,1)}), bf16[4,2,2048]{2,1,0:T(2,128)(2,1)S(1)}, u32[]{:S(2)}, u32[]{:S(2)}) async-start(bf16[4,2,2048]{2,1,0:T(2,128)(2,1)} %reshape.388), calls=%async_computation.4 | async-start | bytes 65536 | tf_op jit(solution)/shard_map/all_to_all | solution.py:170
  91.8 1.8 %while.26 = (s32[]{:T(128)}, f32[2,1,32,32]{3,2,0,1:T(8,128)S(1)}, f32[4,2,1,64,32]{3,4,0,1,2:T(8,128)S(1)}, f32[4,2,1,32]{3,0,1,2:T(4,128)S(1)}, f32[4,2,1,64,3...) while((s32[]{:T(128)}, f32[2,1,32,32]{3,2,0,1:T(8,128)S(1)}, ...), condition=%wide.region_3.4_spmd.clone, body=%wide.region_2.3_spmd.clone.sunk | while | flops 3153923 | bytes 209522 | solution.py:62
  94.0 0.6 convolution_multiply_fusion.1
  96.5 0.7 all-to-all-done.4
  98.5 2.0 %while.27 = (s32[]{:T(128)}, f32[2,1,32,32]{3,2,0,1:T(8,128)S(1)}, f32[4,2,1,64,32]{3,4,0,1,2:T(8,128)S(1)}, f32[4,2,1,32]{3,0,1,2:T(4,128)S(1)}, f32[4,2,1,64,3...) while((s32[]{:T(128)}, f32[2,1,32,32]{3,2,0,1:T(8,128)S(1)}, ...), condition=%wide.region_6.7_spmd.clone, body=%wide.region_5.6_spmd.clone.sunk | while | flops 3153923 | bytes 240763 | solution.py:62
  100.4 0.6 convolution_multiply_fusion
  101.0 0.5 fusion.29
  102.0 0.6 copy-done.8
  102.9 0.8 reshape.390
  103.7 4.5 %all-to-all-start.5 = ((bf16[4,2,2048]{2,1,0:T(2,128)(2,1)}), bf16[4,2,2048]{2,1,0:T(2,128)(2,1)S(1)}, u32[]{:S(2)}, u32[]{:S(2)}) async-start(bf16[4,2,2048]{2,1,0:T(2,128)(2,1)} %reshape.390), calls=%async_computation.5 | async-start | bytes 65536 | tf_op jit(solution)/shard_map/all_to_all | solution.py:183
  108.2 9.0 %all_gather.23 = bf16[128,1024]{1,0:T(8,128)(2,1)S(1)} all-gather(bf16[16,1024]{1,0:T(8,128)(2,1)S(1)} %copy-done.4), channel_id=1, replica_groups=mesh['sp'=4,'dp'=8] {'dp'}, dimensions={0}, use_global_device_ids=true | all-gather | bytes 294912 | tf_op jit(solution)/shard_map/all_gather | solution.py:14
  117.6 1.0 convolution_convert_fusion
  (130 shorter events, 12.0 us)
Async XLA Ops:
  0.0 55.2 %copy-start = (bf16[16,128]{1,0:T(8,128)(2,1)S(1)}, bf16[16,128]{1,0:T(8,128)(2,1)}, u32[]{:S(2)}) copy-start(bf16[16,128]{1,0:T(8,128)(2,1)} %param.24) | copy-start | bytes 12292
  0.0 12.4 %copy-start.1 = (bf16[2,64,1024]{2,1,0:T(8,128)(2,1)S(1)}, bf16[2,64,1024]{2,1,0:T(8,128)(2,1)}, u32[]{:S(2)}) copy-start(bf16[2,64,1024]{2,1,0:T(8,128)(2,1)} %param.17) | copy-start | bytes 786436
  1.3 11.1 %copy-start.5 = (f32[1024]{0:T(1024)S(1)}, f32[1024]{0:T(1024)}, u32[]{:S(2)}) copy-start(f32[1024]{0:T(1024)} %param.18) | copy-start | bytes 12292
  13.6 5.0 %copy-start.6 = (bf16[128,16]{0,1:T(8,128)(2,1)S(1)}, bf16[128,16]{0,1:T(8,128)(2,1)}, u32[]{:S(2)}) copy-start(bf16[128,16]{0,1:T(8,128)(2,1)} %param.22) | copy-start | bytes 12292
  13.6 46.1 %all-to-all-start = ((bf16[4,2,2048]{2,1,0:T(2,128)(2,1)}), bf16[4,2,2048]{2,1,0:T(2,128)(2,1)S(1)}, u32[]{:S(2)}, u32[]{:S(2)}) async-start(bf16[4,2,2048]{2,1,0:T(2,128)(2,1)} %reshape.386), calls=%async_computation | async-start | bytes 65536 | tf_op jit(solution)/shard_map/all_to_all | solution.py:143
  18.6 8.8 %copy-start.2 = (bf16[128,128]{1,0:T(8,128)(2,1)S(1)}, bf16[128,128]{1,0:T(8,128)(2,1)}, u32[]{:S(2)}) copy-start(bf16[128,128]{1,0:T(8,128)(2,1)} %param.20) | copy-start | bytes 98308
  36.5 0.8 copy-start.3
  46.3 0.7 copy-start.7
  47.0 8.2 %copy-start.10 = (f32[128]{0:T(128)S(1)}, f32[128]{0:T(128)}, u32[]{:S(2)}) copy-start(f32[128]{0:T(128)} %param.26) | copy-start | bytes 1540
  55.2 0.7 copy-start.9
  55.2 0.7 copy-start.11
  59.7 10.7 %all-to-all-start.1 = ((bf16[4,2,2048]{2,1,0:T(2,128)(2,1)}), bf16[4,2,2048]{2,1,0:T(2,128)(2,1)S(1)}, u32[]{:S(2)}, u32[]{:S(2)}) async-start(bf16[4,2,2048]{2,1,0:T(2,128)(2,1)} %reshape.382), calls=%async_computation.1 | async-start | bytes 65536 | tf_op jit(solution)/shard_map/all_to_all | solution.py:163
  70.5 8.9 %all-to-all-start.3 = ((bf16[4,2,2048]{2,1,0:T(2,128)(2,1)}), bf16[4,2,2048]{2,1,0:T(2,128)(2,1)S(1)}, u32[]{:S(2)}, u32[]{:S(2)}) async-start(bf16[4,2,2048]{2,1,0:T(2,128)(2,1)} %reshape.380), calls=%async_computation.3 | async-start | bytes 65536 | tf_op jit(solution)/shard_map/all_to_all | solution.py:148
  79.4 8.9 %all-to-all-start.2 = ((bf16[4,2,2048]{2,1,0:T(2,128)(2,1)}), bf16[4,2,2048]{2,1,0:T(2,128)(2,1)S(1)}, u32[]{:S(2)}, u32[]{:S(2)}) async-start(bf16[4,2,2048]{2,1,0:T(2,128)(2,1)} %reshape.384), calls=%async_computation.2 | async-start | bytes 65536 | tf_op jit(solution)/shard_map/all_to_all | solution.py:145
  88.3 8.9 %all-to-all-start.4 = ((bf16[4,2,2048]{2,1,0:T(2,128)(2,1)}), bf16[4,2,2048]{2,1,0:T(2,128)(2,1)S(1)}, u32[]{:S(2)}, u32[]{:S(2)}) async-start(bf16[4,2,2048]{2,1,0:T(2,128)(2,1)} %reshape.388), calls=%async_computation.4 | async-start | bytes 65536 | tf_op jit(solution)/shard_map/all_to_all | solution.py:170
  102.0 0.7 copy-start.8
  103.7 4.5 %copy-start.4 = (bf16[16,1024]{1,0:T(8,128)(2,1)S(1)}, bf16[16,1024]{1,0:T(8,128)(2,1)}, u32[]{:S(2)}) copy-start(bf16[16,1024]{1,0:T(8,128)(2,1)} %param.29) | copy-start | bytes 98308
  103.7 13.6 %all-to-all-start.5 = ((bf16[4,2,2048]{2,1,0:T(2,128)(2,1)}), bf16[4,2,2048]{2,1,0:T(2,128)(2,1)S(1)}, u32[]{:S(2)}, u32[]{:S(2)}) async-start(bf16[4,2,2048]{2,1,0:T(2,128)(2,1)} %reshape.390), calls=%async_computation.5 | async-start | bytes 65536 | tf_op jit(solution)/shard_map/all_to_all | solution.py:183
